TPU v7x, 512 devices: a whole 4x8x8 slice. The times are simulated.
512 devices in a mesh: kv: 64 (over z, y), tp: 8 (over x, core).
Axes of the slice: x: 4, y: 8, z: 8, core: 2. Of those that a mesh axis runs over, the one named last changes fastest.
Arguments:
- hidden_in: bfloat16 [8, 1024], P(None, 'tp'), may hold values from -18 to 18, as said below
- input_gain: float32 [1024], P('tp'), may hold values from 0.1 to 1.9
- down_query: bfloat16 [1024, 256], P('tp'), may hold values from -0.1875 to 0.1875
- down_latent: bfloat16 [1024, 256], P('tp'), may hold values from -0.1875 to 0.1875
- down_rope: bfloat16 [1024, 64], P('tp'), may hold values from -0.1875 to 0.1875
- query_gain: float32 [256], replicated, may hold values from 0.1 to 1.9
- latent_gain: float32 [256], replicated, may hold values from 0.1 to 1.9
- up_query: bfloat16 [256, 8, 128], P(None, 'tp'), may hold values from -0.375 to 0.375
- up_rope: bfloat16 [256, 8, 64], P(None, 'tp'), may hold values from -0.375 to 0.375
- key_up: bfloat16 [256, 8, 128], P(None, 'tp'), may hold values from -0.375 to 0.375
- value_up: bfloat16 [256, 8, 128], P(None, 'tp'), may hold values from -0.375 to 0.375
- out_proj: bfloat16 [1024, 1024], P('tp', 'kv'), may hold values from -2 to 2, as said below
- output_gain: float32 [1024], P('kv'), may hold values from 0.1 to 1.9
- latent_cache: bfloat16 [8, 65536, 256], P(None, ('kv', 'tp')), may hold values from -6 to 6
- rope_cache: bfloat16 [8, 65536, 64], P(None, ('kv', 'tp')), may hold values from -6 to 6
- lengths: int32 [8], replicated, may hold values from 1 to 65536, as said below
Outputs:
- mixed: bfloat16 [8, 1024], P(None, 'kv')
Inputs may be any that keep to these rules, and one draw needn't show every extreme that they name: Each length lies between 1 and 65536; in every draw some sequence has exactly 65536 and some exactly 1; lengths are heavily skewed toward short ones. `hidden_in`: activations whose size differs strongly between blocks of 64 features, by sequence. `out_proj`: output projection whose columns differ strongly in size.
All inputs are finite; a program needn't handle non-finite values.
Results may differ from a plain program's by a relative error of at most 0.015.
Values may be sent and summed in bfloat16 or wider, within the bound.
A program may use at most 128 MiB of HBM per device.

v0:
```python
import math

import jax
import jax.numpy as jnp
from jax import lax
from jax.sharding import Mesh
from jax.sharding import PartitionSpec as P

D = 1024
DN = 128
DR = 64
TP = ("tp_0", "tp_1")
KV_TP = ("kv_0", "kv_1", "tp_0", "tp_1")
KV = ("kv_0", "kv_1")


THETA = 10000.0
EPSILON = 1e-06


def joined_along(pieces, dim):
    shape = list(pieces.shape[1:])
    shape[dim] *= pieces.shape[0]
    return jnp.moveaxis(pieces, 0, dim).reshape(shape)


def one_gather(arrays, axis, dims):
    line = jnp.concatenate([a.reshape(-1) for a in arrays])
    lines, at, finished = lax.all_gather(line, axis), 0, []
    for a, dim in zip(arrays, dims):
        pieces = lines[:, at : at + a.size].reshape(-1, *a.shape)
        finished.append(joined_along(pieces, dim))
        at += a.size
    return tuple(finished)


def combined_by_axis(x, axes, combine):
    for axis in axes:
        pieces = jax.tree.map(lambda part: lax.all_gather(part, axis), x)
        x = jax.tree.map(lambda part: part[0], pieces)
        for k in range(1, lax.axis_size(axis)):
            x = combine(x, jax.tree.map(lambda part: part[k], pieces))
    return x


def over_axes(x, axes):
    for axis in axes:
        x = lax.psum(x, axis)
    return x


def rotate(values, angles):
    half_width = values.shape[-1] // 2
    first_half = values[..., :half_width]
    second_half = values[..., half_width:]
    cosine = jnp.cos(angles)
    sine_part = jnp.sin(angles)
    return jnp.concatenate(
        [
            first_half * cosine - second_half * sine_part,
            second_half * cosine + first_half * sine_part,
        ],
        axis=-1,
    )


def angles_for(positions, rot_width):
    inverse = 1.0 / THETA ** (jnp.arange(0, rot_width, 2, dtype=jnp.float32) / rot_width)
    return positions[:, None] * inverse[None, :]


def normed(values, gain_row):
    return (
        values
        * lax.rsqrt(jnp.mean(values * values, axis=-1, keepdims=True) + EPSILON)
        * gain_row.astype(jnp.float32)
    )


def combine(earlier, later):
    highest = jnp.maximum(earlier[0], later[0])
    from_early = jnp.exp(earlier[0] - highest)
    from_late = jnp.exp(later[0] - highest)
    return (
        highest,
        earlier[1] * from_early + later[1] * from_late,
        earlier[2] * from_early[..., None] + later[2] * from_late[..., None],
    )


def body(
    hidden_in,
    input_gain,
    down_query,
    down_latent,
    down_rope,
    query_gain,
    latent_gain,
    up_query,
    up_rope,
    key_up,
    value_up,
    out_proj,
    output_gain,
    latent_cache,
    rope_cache,
    lengths,
):
    floats = hidden_in.astype(jnp.float32)
    scaled = (floats * input_gain.astype(jnp.float32)).astype(jnp.bfloat16)
    local_sq = jnp.sum(floats * floats, axis=1)
    part_query = jnp.dot(scaled, down_query, preferred_element_type=jnp.float32)
    part_latent = jnp.dot(scaled, down_latent, preferred_element_type=jnp.float32)
    part_rope = jnp.dot(scaled, down_rope, preferred_element_type=jnp.float32)
    total_sq, query_low, latent_low, rope_low = lax.psum(
        (local_sq, part_query, part_latent, part_rope), TP
    )
    inv_rms = lax.rsqrt(total_sq / D + EPSILON)[:, None]
    query_low = query_low * inv_rms
    latent_low = latent_low * inv_rms
    rope_low = rope_low * inv_rms
    positions = lengths.astype(jnp.float32)
    query_normed = normed(query_low, query_gain).astype(jnp.bfloat16)
    query_nope = jnp.einsum(
        "bq,qhd->bhd", query_normed, up_query, preferred_element_type=jnp.float32
    ).astype(jnp.bfloat16)
    query_rope = jnp.einsum(
        "bq,qhr->bhr", query_normed, up_rope, preferred_element_type=jnp.float32
    )
    query_rope = rotate(query_rope, angles_for(positions, DR)[:, None, :]).astype(jnp.bfloat16)
    latent_heads = jnp.einsum(
        "bhd,chd->bhc", query_nope, key_up, preferred_element_type=jnp.float32
    ).astype(jnp.bfloat16)
    latent_query, rope_query = one_gather((latent_heads, query_rope), TP, (1, 1))
    latent_new = normed(latent_low, latent_gain).astype(jnp.bfloat16)
    rope_new = rotate(rope_low, angles_for(positions, DR)).astype(jnp.bfloat16)
    span_len = latent_cache.shape[1]
    offset = lax.axis_index(KV_TP) * span_len
    places = offset + jnp.arange(span_len, dtype=jnp.int32)
    usable = (places[None, :] < lengths[:, None])[:, None, :]
    factor = 1.0 / math.sqrt(DN + DR)
    scores = (
        jnp.einsum("bhc,bpc->bhp", latent_query, latent_cache, preferred_element_type=jnp.float32)
        + jnp.einsum("bhr,bpr->bhp", rope_query, rope_cache, preferred_element_type=jnp.float32)
    ) * factor
    scores = jnp.where(usable, scores, -1e30)
    local_top = jnp.max(scores, axis=-1)
    weights = jnp.where(usable, jnp.exp(scores - local_top[..., None]), 0.0)
    local_mass = jnp.sum(weights, axis=-1)
    local_sum = jnp.einsum(
        "bhp,bpc->bhc",
        weights.astype(jnp.bfloat16),
        latent_cache,
        preferred_element_type=jnp.float32,
    )
    highest, total_mass, summed = combined_by_axis(
        (local_top, local_mass, local_sum), KV_TP, combine
    )
    latent_wide = latent_new.astype(jnp.float32)
    new_score = (
        jnp.sum(latent_query.astype(jnp.float32) * latent_wide[:, None, :], axis=-1)
        + jnp.sum(
            rope_query.astype(jnp.float32) * rope_new.astype(jnp.float32)[:, None, :], axis=-1
        )
    ) * factor
    final_top = jnp.maximum(highest, new_score)
    keep_old = jnp.exp(highest - final_top)
    fresh_weight = jnp.exp(new_score - final_top)
    total_mass = total_mass * keep_old + fresh_weight
    summed = summed * keep_old[..., None] + fresh_weight[..., None] * latent_wide[:, None, :]
    attended = (summed / total_mass[..., None]).astype(jnp.bfloat16)
    heads_dev = value_up.shape[1]
    own_heads = lax.dynamic_slice_in_dim(attended, lax.axis_index(TP) * heads_dev, heads_dev, 1)
    values_out = jnp.einsum(
        "bhc,chv->bhv", own_heads, value_up, preferred_element_type=jnp.float32
    ).astype(jnp.bfloat16)
    flattened = values_out.reshape(values_out.shape[0], heads_dev * values_out.shape[2])
    out_part = jnp.dot(flattened, out_proj, preferred_element_type=jnp.float32)
    out_cols = lax.psum(out_part, TP)
    out_sq = over_axes(jnp.sum(out_cols * out_cols, axis=1), KV)
    out_rms = lax.rsqrt(out_sq / D + EPSILON)[:, None]
    return (out_cols * out_rms * output_gain.astype(jnp.float32)).astype(jnp.bfloat16)


def solution(mesh):
    split = Mesh(mesh.devices.reshape(8, 8, 4, 2), ("kv_0", "kv_1", "tp_0", "tp_1"))
    in_specs = (
        P(None, TP),
        P(TP),
        P(TP, None),
        P(TP, None),
        P(TP, None),
        P(),
        P(),
        P(None, TP, None),
        P(None, TP, None),
        P(None, TP, None),
        P(None, TP, None),
        P(TP, KV),
        P(KV),
        P(None, KV_TP, None),
        P(None, KV_TP, None),
        P(),
    )
    out_specs = P(None, KV)
    return jax.shard_map(body, mesh=split, in_specs=in_specs, out_specs=out_specs, check_vma=False)
```

profile of v0, /device:TPU:1, one launch (start us, length us, event | category | flops | bytes accessed | tf_op | source)
XLA Modules:
  0.0 286.4 jit_solution(13058574378022712312)
XLA Ops:
  0.1 0.8 broadcast_compare_fusion
  0.8 0.7 convert_element_type.82
  1.5 0.8 fusion.68
  2.3 0.9 fusion.163
  3.2 0.1 fusion.167
  3.3 0.1 fusion.165
  3.5 26.9 %all-reduce = (f32[8,256]{1,0:T(8,128)S(1)}, f32[8,256]{1,0:T(8,128)S(1)}, f32[8]{0:T(128)S(1)}, f32[8,64]{1,0:T(8,128)S(1)}) all-reduce(f32[8,256]{1,0:T(8,128)S(1)} %fusion.167, f32[8,256]{1,0:T(8,128)S(1)} %fusion.165, f32[8]{0:T(128)S(1)} %fusion.68, ...), channel_id=1, replica_groups=mesh['kv_0'=8,'kv_1'=8,'tp_0'=4,'tp_1'=2] {'tp_0','tp_1'}, use_global_device_ids=true, to_apply=%region_0.0 | all-reduce | flops 4616 | bytes 36928 | tf_op jit(solution)/shard_map/psum | solution.py:115
  30.4 0.1 fusion.70
  30.6 0.2 multiply_reduce_fusion.2
  30.8 0.7 copy-done.8
  31.6 0.2 convolution_bitcast_fusion
  31.8 0.6 copy-done.11
  32.4 0.3 fusion.2
  32.7 0.1 fusion.74
  32.9 0.1 convert_element_type.83
  33.0 16.1 %all-gather.4 = bf16[8,1,2560]{2,1,0:T(2,128)(2,1)S(1)} all-gather(bf16[1,1,2560]{2,1,0:T(2,128)(2,1)S(1)} %reshape.968), channel_id=2, replica_groups=mesh['kv_0'=8,'kv_1'=8,'tp_0'=4,'tp_1'=2] {'tp_0','tp_1'}, dimensions={0}, use_global_device_ids=true | all-gather | bytes 46080 | tf_op jit(solution)/shard_map/all_gather | solution.py:29
  49.2 0.1 multiply_reduce_fusion
  49.3 0.2 fusion.173
  49.5 0.1 reshape.928
  49.6 0.1 multiply_reduce_fusion.1
  49.7 0.5 copy-done.1
  50.2 0.2 fusion.172
  50.4 0.2 fusion.49
  50.6 21.2 %all-gather.3 = f32[64,8]{1,0:T(8,128)S(1)} all-gather(f32[8,8]{1,0:T(8,128)S(1)} %fusion.49), channel_id=5, replica_groups=mesh['kv_0'=8,'kv_1'=8,'tp_0'=4,'tp_1'=2] {'kv_0'}, dimensions={0}, use_global_device_ids=true | all-gather | bytes 2304 | tf_op jit(solution)/shard_map/all_gather | solution.py:39
  71.8 0.2 fusion.51
  72.0 18.1 %all-gather.2 = f32[64,8]{1,0:T(8,128)S(1)} all-gather(f32[8,8]{1,0:T(8,128)S(1)} %get-tuple-element.77), channel_id=4, replica_groups=mesh['kv_0'=8,'kv_1'=8,'tp_0'=4,'tp_1'=2] {'kv_0'}, dimensions={0}, use_global_device_ids=true | all-gather | bytes 2304 | tf_op jit(solution)/shard_map/all_gather | solution.py:39
  90.2 19.7 %all_gather.74 = f32[8,8,8]{2,1,0:T(8,128)S(1)} all-gather(f32[1,8,8]{2,1,0:T(8,128)S(1)} %get-tuple-element.20), channel_id=1, replica_groups=mesh['kv_0'=8,'kv_1'=8,'tp_0'=4,'tp_1'=2] {'kv_1'}, dimensions={0}, use_global_device_ids=true | all-gather | bytes 2304 | tf_op jit(solution)/shard_map/all_gather | solution.py:39
  109.9 18.1 %all_gather.67 = f32[8,8,8]{2,1,0:T(8,128)S(1)} all-gather(f32[1,8,8]{2,1,0:T(8,128)S(1)} %get-tuple-element.21), channel_id=1, replica_groups=mesh['kv_0'=8,'kv_1'=8,'tp_0'=4,'tp_1'=2] {'kv_1'}, dimensions={0}, use_global_device_ids=true | all-gather | bytes 2304 | tf_op jit(solution)/shard_map/all_gather | solution.py:39
  128.1 8.9 %all_gather.75 = f32[4,8,8]{2,1,0:T(8,128)S(1)} all-gather(f32[1,8,8]{2,1,0:T(8,128)S(1)} %get-tuple-element.18), channel_id=1, replica_groups=mesh['kv_0'=8,'kv_1'=8,'tp_0'=4,'tp_1'=2] {'tp_0'}, dimensions={0}, use_global_device_ids=true | all-gather | bytes 1280 | tf_op jit(solution)/shard_map/all_gather | solution.py:39
  137.0 8.9 %all_gather.69 = f32[4,8,8]{2,1,0:T(8,128)S(1)} all-gather(f32[1,8,8]{2,1,0:T(8,128)S(1)} %get-tuple-element.19), channel_id=1, replica_groups=mesh['kv_0'=8,'kv_1'=8,'tp_0'=4,'tp_1'=2] {'tp_0'}, dimensions={0}, use_global_device_ids=true | all-gather | bytes 1280 | tf_op jit(solution)/shard_map/all_gather | solution.py:39
  146.0 32.9 %all_gather.76 = f32[2,8,8]{2,1,0:T(8,128)S(1)} all-gather(f32[1,8,8]{2,1,0:T(8,128)S(1)} %get-tuple-element.16), channel_id=1, replica_groups=mesh['kv_0'=8,'kv_1'=8,'tp_0'=4,'tp_1'=2] {'tp_1'}, dimensions={0}, use_global_device_ids=true | all-gather | bytes 768 | tf_op jit(solution)/shard_map/all_gather | solution.py:39
  178.8 1.8 all_gather.71
  181.0 19.3 %all-gather.1 = f32[64,8,256]{2,1,0:T(8,128)S(1)} all-gather(f32[8,8,256]{2,1,0:T(8,128)S(1)} %fusion.51), channel_id=3, replica_groups=mesh['kv_0'=8,'kv_1'=8,'tp_0'=4,'tp_1'=2] {'kv_0'}, dimensions={0}, use_global_device_ids=true | all-gather | bytes 589824 | tf_op jit(solution)/shard_map/all_gather | solution.py:39
  200.2 0.2 fusion.23
  200.4 19.3 %all_gather.66 = f32[8,8,8,256]{3,2,1,0:T(8,128)S(1)} all-gather(f32[1,8,8,256]{3,2,1,0:T(8,128)S(1)} %fusion.23), channel_id=1, replica_groups=mesh['kv_0'=8,'kv_1'=8,'tp_0'=4,'tp_1'=2] {'kv_1'}, dimensions={0}, use_global_device_ids=true | all-gather | bytes 589824 | tf_op jit(solution)/shard_map/all_gather | solution.py:39
  219.7 0.2 fusion.9
  219.9 9.7 %all_gather.68 = f32[4,8,8,256]{3,2,1,0:T(8,128)S(1)} all-gather(f32[1,8,8,256]{3,2,1,0:T(8,128)S(1)} %fusion.9), channel_id=1, replica_groups=mesh['kv_0'=8,'kv_1'=8,'tp_0'=4,'tp_1'=2] {'tp_0'}, dimensions={0}, use_global_device_ids=true | all-gather | bytes 327680 | tf_op jit(solution)/shard_map/all_gather | solution.py:39
  229.5 0.1 fusion.4
  229.7 17.0 %all_gather.70 = f32[2,8,8,256]{3,2,1,0:T(8,128)S(1)} all-gather(f32[1,8,8,256]{3,2,1,0:T(8,128)S(1)} %fusion.4), channel_id=1, replica_groups=mesh['kv_0'=8,'kv_1'=8,'tp_0'=4,'tp_1'=2] {'tp_1'}, dimensions={0}, use_global_device_ids=true | all-gather | bytes 196608 | tf_op jit(solution)/shard_map/all_gather | solution.py:39
  246.7 0.1 divide_convert_fusion
  246.8 0.7 copy-done.4
  247.5 0.2 fusion.3
  247.7 12.1 %psum.53 = f32[8,16]{1,0:T(8,128)S(1)} all-reduce(f32[8,16]{1,0:T(8,128)S(1)} %fusion.3), channel_id=1, replica_groups=mesh['kv_0'=8,'kv_1'=8,'tp_0'=4,'tp_1'=2] {'tp_0','tp_1'}, use_global_device_ids=true, to_apply=%region_11.12 | all-reduce | flops 128 | bytes 1024 | tf_op jit(solution)/shard_map/psum | solution.py:179
  259.8 0.1 multiply_reduce_fusion.4
  259.9 13.0 %psum.54 = f32[8]{0:T(128)S(1)} all-reduce(f32[8]{0:T(128)S(1)} %multiply_reduce_fusion.4), channel_id=1, replica_groups=mesh['kv_0'=8,'kv_1'=8,'tp_0'=4,'tp_1'=2] {'kv_0'}, use_global_device_ids=true, to_apply=%region_13.14 | all-reduce | flops 8 | bytes 64 | tf_op jit(solution)/shard_map/psum | solution.py:48
  272.9 12.2 %psum.55 = f32[8]{0:T(128)S(1)} all-reduce(f32[8]{0:T(128)S(1)} %psum.54), channel_id=1, replica_groups=mesh['kv_0'=8,'kv_1'=8,'tp_0'=4,'tp_1'=2] {'kv_1'}, use_global_device_ids=true, to_apply=%region_14.15 | all-reduce | flops 8 | bytes 64 | tf_op jit(solution)/shard_map/psum | solution.py:48
  285.1 0.6 copy-done.9
  285.7 0.6 multiply_convert_fusion.2
  (57 shorter events, 0.9 us)
Async XLA Ops:
  0.0 49.3 %copy-start = (bf16[8,128,256]{2,1,0:T(8,128)(2,1)S(1)}, bf16[8,128,256]{2,1,0:T(8,128)(2,1)}, u32[]{:S(2)}) copy-start(bf16[8,128,256]{2,1,0:T(8,128)(2,1)} %param.29) | copy-start | bytes 1572868
  0.0 3.2 %copy-start.2 = (bf16[128,256]{1,0:T(8,128)(2,1)S(1)}, bf16[128,256]{1,0:T(8,128)(2,1)}, u32[]{:S(2)}) copy-start(bf16[128,256]{1,0:T(8,128)(2,1)} %param.18) | copy-start | bytes 196612
  0.0 3.2 %copy-start.5 = (bf16[8,128]{1,0:T(8,128)(2,1)S(1)}, bf16[8,128]{1,0:T(8,128)(2,1)}, u32[]{:S(2)}) copy-start(bf16[8,128]{1,0:T(8,128)(2,1)} %param.16) | copy-start | bytes 6148
  0.0 3.2 %copy-start.6 = (f32[128]{0:T(128)S(1)}, f32[128]{0:T(128)}, u32[]{:S(2)}) copy-start(f32[128]{0:T(128)} %param.17) | copy-start | bytes 1540
  0.0 3.3 %copy-start.3 = (bf16[128,256]{1,0:T(8,128)(2,1)S(1)}, bf16[128,256]{1,0:T(8,128)(2,1)}, u32[]{:S(2)}) copy-start(bf16[128,256]{1,0:T(8,128)(2,1)} %param.19) | copy-start | bytes 196612
  30.4 1.2 copy-start.12
  30.8 0.8 copy-start.13
  30.8 0.7 copy-start.8
  31.5 0.8 copy-start.11
  31.6 0.8 copy-start.10
  49.3 0.9 copy-start.1
  246.6 0.8 copy-start.4
  246.6 0.8 copy-start.7
  285.1 0.7 copy-start.9
where the time goes:
time: 292 us; the launch traced here: 286 us
  blocking collectives  275 us (94%)
  other arithmetic  4.91 us (2%)
  local copies, waits for them, and re-layouts  3.63 us (1%)
    all_gather x12, blocking collectives, combined_by_axis(): pieces = jax.tree.map(lambda part: lax.all_gather(part, axis), x)  195 us
    psum x1, blocking collectives, body(): lax.psum((local_sq, part_query, part_latent, part_rope), TP)  26.9 us
    psum x2, blocking collectives, over_axes(): x = lax.psum(x, axis)  25.1 us
    all_gather x1, blocking collectives, one_gather(): lines, at, finished = (lax.all_gather(line, axis), 0, [])  16.1 us
    psum x1, blocking collectives, body(): out_cols = lax.psum(out_part, TP)  12.1 us

commit v1 on v0

v1 whole, which is shorter than its diff:
```python
import functools
import math

import jax
import jax.numpy as jnp
from jax import lax
from jax.experimental import pallas as pl
from jax.experimental.pallas import tpu as pltpu
from jax.sharding import Mesh
from jax.sharding import PartitionSpec as P

D = 1024
DN = 128
DR = 64
THETA = 10000.0
EPSILON = 1e-06
FACTOR = 1.0 / math.sqrt(DN + DR)
LOW = -1e30
TP = ("x", "c")
KV = ("z", "y")
KV_TP = ("z", "y", "x", "c")
MESH = pl.DeviceIdType.MESH
F32 = jnp.float32
BF16 = jnp.bfloat16

TP_ORDER = (4, 5, 2, 3, 6, 7, 1)
RING_ORDER = (4, 3, 5, 2, 6, 1, 7)


def mirrored(slot):
    dx, dc = slot // 2, slot % 2
    return ((4 - dx) % 4) * 2 + dc


def dot(a, b, dims):
    return lax.dot_general(a, b, (dims, ((), ())), preferred_element_type=F32)


def iota(shape, dim):
    return lax.broadcasted_iota(jnp.int32, shape, dim)


def cos_sin(angle):
    turns = jnp.floor(angle * (2.0 / math.pi) + 0.5)
    r = angle - turns * 1.5703125
    r = r - turns * 4.825592041015625e-4
    r = r - turns * 1.2675907950567e-6
    r2 = r * r
    sine = r + r * r2 * (-1 / 6 + r2 * (1 / 120 + r2 * (-1 / 5040 + r2 * (1 / 362880))))
    cosine = 1.0 + r2 * (
        -0.5 + r2 * (1 / 24 + r2 * (-1 / 720 + r2 * (1 / 40320 + r2 * (-1 / 3628800))))
    )
    quadrant = turns - 4.0 * jnp.floor(turns * 0.25)
    odd = (quadrant == 1.0) | (quadrant == 3.0)
    c = jnp.where(odd, sine, cosine)
    s = jnp.where(odd, cosine, sine)
    c = jnp.where((quadrant == 1.0) | (quadrant == 2.0), -c, c)
    s = jnp.where((quadrant == 2.0) | (quadrant == 3.0), -s, s)
    return c, s


def split_lanes(value, rows):
    wide = jnp.broadcast_to(value, (rows, 128))
    high = wide.astype(BF16).astype(F32)
    rest = wide - high
    mid = rest.astype(BF16).astype(F32)
    low = rest - mid
    lane = iota((rows, 128), 1)
    return jnp.where(lane < 32, high, jnp.where(lane < 64, mid, low)).astype(BF16)


def joined_lanes(block):
    wide = block.astype(F32)
    return wide[:, 0:1] + wide[:, 32:33] + wide[:, 64:65]


def merged(parts):
    top = parts[0][1]
    for _, lse in parts[1:]:
        top = jnp.maximum(top, lse)
    weights = [jnp.exp(lse - top) for _, lse in parts]
    mass = weights[0]
    for w in weights[1:]:
        mass = mass + w
    total = parts[0][0] * weights[0]
    for (values, _), w in zip(parts[1:], weights[1:]):
        total = total + values * w
    return total * (1.0 / mass), top + jnp.log(mass)


def kernel(
    lengths,
    hidden_h, igain_h, dq_h, dl_h, dr_h, qgain_h, lgain_h, uq_h, ur_h, ku_h, vu_h, op_h, ogain_h, lat_h, rop_h,
    out,
    hidden, igain, dq, dl, dr, qgain, lgain, uq, ur, ku, vu, ogain, lat, rop,
    s1, r1, s1b, r1b, s2, r2, s3, r3, s4, r4, s5, r5, s6, r6, wt,
    load_sem, send_sem, recv_sem,
):
    z, y, x, c = (lax.axis_index(a) for a in KV_TP)
    me = x * 2 + c

    def tp_peer(slot):
        dx, dc = slot // 2, slot % 2
        return {"x": lax.rem(x + dx, 4), "c": lax.rem(c + dc, 2)}

    def y_peer(d):
        return {"y": lax.rem(y + d, 8)}

    def z_peer(d):
        return {"z": lax.rem(z + d, 8)}

    barrier = pltpu.get_barrier_semaphore()
    for slot in TP_ORDER:
        pl.semaphore_signal(barrier, inc=1, device_id=tp_peer(slot), device_id_type=MESH)
    for d in RING_ORDER:
        pl.semaphore_signal(barrier, inc=1, device_id=y_peer(d), device_id_type=MESH)
        pl.semaphore_signal(barrier, inc=1, device_id=z_peer(d), device_id_type=MESH)

    pairs = (
        (hidden_h, hidden), (igain_h, igain), (dq_h, dq), (dl_h, dl), (dr_h, dr), (op_h, wt.at[0, 0]),
        (qgain_h, qgain), (lgain_h, lgain), (uq_h, uq), (ur_h, ur), (ku_h, ku), (lat_h, lat), (rop_h, rop),
        (vu_h, vu), (ogain_h, ogain),
    )
    loads = {}
    for i, (src, dst) in enumerate(pairs):
        loads[i] = pltpu.make_async_copy(src, dst, load_sem.at[i])
        loads[i].start()

    sent = []

    def copy(phase, src, dst, send_slot, recv_slot, peer):
        return pltpu.make_async_remote_copy(
            src_ref=src,
            dst_ref=dst,
            send_sem=send_sem.at[phase, send_slot],
            recv_sem=recv_sem.at[phase, recv_slot],
            device_id=peer,
            device_id_type=MESH,
        )

    def tp_start(phase, src, dst):
        for slot in TP_ORDER:
            there = mirrored(slot)
            one = copy(phase, src(slot), dst(there), slot, there, tp_peer(slot))
            one.start()
            sent.append(one)

    def ring_start(phase, src, dst, peer):
        for d in RING_ORDER:
            there = 8 - d
            one = copy(phase, src, dst(there), d, there, peer(d))
            one.start()
            sent.append(one)

    def wait(phase, dst, order):
        for slot in order:
            copy(phase, dst(slot), dst(slot), slot, slot, tp_peer(1)).wait_recv()

    for i in (0, 1, 2):
        loads[i].wait()
    floats = hidden[...].astype(F32)
    scaled = (floats * igain[...]).astype(BF16)
    square = jnp.sum(floats * floats, axis=1, keepdims=True)
    s1[:, 0:256] = dot(scaled, dq[...], ((1,), (0,))).astype(BF16)
    s1[:, 256:384] = split_lanes(square, 8)
    for i in (3, 4):
        loads[i].wait()
    s1b[:, 0:256] = dot(scaled, dl[...], ((1,), (0,))).astype(BF16)
    rope_down = jnp.concatenate([dr[...], dr[...]], axis=0)
    s1b[:, 256:384] = dot(scaled, rope_down, ((1,), (1,))).astype(BF16)
    loads[5].wait()

    row = iota((8, 128), 0)
    lane = iota((8, 128), 1)
    length = jnp.zeros((8, 128), jnp.int32)
    for b in range(8):
        length = jnp.where(row == b, lengths[b], length)
    frequency = jnp.zeros((8, 128), F32)
    within = lax.rem(lane, 32)
    for i in range(32):
        frequency = jnp.where(within == i, float(THETA ** (-2.0 * i / DR)), frequency)
    cosine, sine = cos_sin(length.astype(F32) * frequency)
    sine = jnp.where(lax.rem(lane, 64) < 32, -sine, sine)

    def rotated(doubled):
        return doubled * cosine + pltpu.roll(doubled, 32, 1) * sine

    pl.semaphore_wait(barrier, 21)
    tp_start(0, lambda slot: s1, lambda slot: r1.at[slot])
    tp_start(1, lambda slot: s1b, lambda slot: r1b.at[slot])
    ring_start(2, wt.at[0, 0], lambda d: wt.at[0, d], y_peer)

    r1[0] = s1[...]
    r1b[0] = s1b[...]
    for i in (6, 7, 8, 9, 10):
        loads[i].wait()
    wait(0, lambda slot: r1.at[slot], TP_ORDER[::-1])
    total = r1[0, :, 0:384].astype(F32)
    for slot in range(1, 8):
        total = total + r1[slot].astype(F32)
    inv_rms = lax.rsqrt(joined_lanes(total[:, 256:384]) / D + EPSILON)

    def normed(values, gain):
        return values * lax.rsqrt(jnp.mean(values * values, axis=1, keepdims=True) + EPSILON) * gain

    query = normed(total[:, 0:256] * inv_rms, qgain[...]).astype(BF16)
    nope = dot(query, uq[...], ((1,), (0,))).astype(BF16)
    rope_up = jnp.concatenate([ur[...], ur[...]], axis=0)
    rope = rotated(dot(query, rope_up, ((1,), (1,)))).astype(BF16)
    latent = dot(nope, ku[...], ((1,), (1,))).astype(BF16)
    s2[:, 0:256] = latent
    s2[:, 256:384] = rope
    tp_start(3, lambda slot: s2, lambda slot: r2.at[slot])
    r2[0] = s2[...]

    wait(1, lambda slot: r1b.at[slot], TP_ORDER[::-1])
    fresh = r1b[0].astype(F32)
    for slot in range(1, 8):
        fresh = fresh + r1b[slot].astype(F32)
    fresh = fresh * inv_rms
    latent_new = normed(fresh[:, 0:256], lgain[...]).astype(BF16).astype(F32)
    rope_new = rotated(fresh[:, 256:384]).astype(BF16).astype(F32)
    new_score = jnp.sum(latent.astype(F32) * latent_new, axis=1, keepdims=True)
    new_score = new_score + jnp.sum(
        jnp.where(lane < 64, rope.astype(F32) * rope_new, 0.0), axis=1, keepdims=True
    )
    first_row = (z + y) == 0
    new_score = jnp.where(first_row, new_score * FACTOR, LOW)
    wait(2, lambda d: wt.at[0, d], RING_ORDER[::-1])
    ring_start(4, wt.at[0], lambda d: wt.at[d], z_peer)
    for i in (11, 12, 13, 14):
        loads[i].wait()

    wait(3, lambda slot: r2.at[slot], TP_ORDER[::-1])
    queries = r2[...].reshape(64, 384)
    keys = lat[...].reshape(1024, 256)
    rope_keys = jnp.concatenate([rop[b] for b in range(8)], axis=1)
    every = dot(queries[:, 0:256], keys, ((1,), (1,))) + dot(queries[:, 256:320], rope_keys, ((1,), (0,)))
    row64 = lax.rem(iota((64, 128), 0), 8)
    scores = every[:, 0:128]
    for b in range(1, 8):
        scores = jnp.where(row64 == b, every[:, b * 128 : (b + 1) * 128], scores)
    place = ((z * 8 + y) * 8 + me) * 128 + iota((64, 128), 1)
    usable = place < jnp.concatenate([length] * 8, axis=0)
    scores = jnp.where(usable, scores * FACTOR, LOW)
    top = jnp.max(scores, axis=1, keepdims=True)
    weights = jnp.where(usable, jnp.exp(scores - top), 0.0)
    mass = jnp.sum(weights, axis=1, keepdims=True)
    spread = jnp.concatenate([jnp.where(row64 == b, weights, 0.0).astype(BF16) for b in range(8)], axis=1)
    summed = dot(spread, keys, ((1,), (0,)))
    some = mass > 0.0
    safe = jnp.where(some, mass, 1.0)
    summed = summed * (1.0 / safe)
    lse = jnp.where(some, top + jnp.log(safe), LOW)
    split = split_lanes(lse, 64)
    for slot in range(8):
        s3[slot, :, 0:256] = summed[slot * 8 : slot * 8 + 8].astype(BF16)
        s3[slot, :, 256:384] = split[slot * 8 : slot * 8 + 8]
    tp_start(5, lambda slot: s3.at[slot], lambda slot: r3.at[slot])
    r3[0] = s3[0]

    wait(5, lambda slot: r3.at[slot], TP_ORDER[::-1])
    parts = [(latent_new, new_score)]
    for slot in range(8):
        parts.append((r3[slot, :, 0:256].astype(F32), joined_lanes(r3[slot, :, 256:384])))
    attended, lse = merged(parts)
    values = dot(attended.astype(BF16), vu[...], ((1,), (0,)))

    def ring_merge(phase, values, lse, send, recv, peer):
        send[:, 0:128] = values.astype(BF16)
        send[:, 128:256] = split_lanes(lse, 8)
        ring_start(phase, send, lambda d: recv.at[d], peer)
        recv[0] = send[...]
        wait(phase, lambda d: recv.at[d], RING_ORDER[::-1])
        return merged([(recv[d, :, 0:128].astype(F32), joined_lanes(recv[d, :, 128:256])) for d in range(8)])

    values, lse = ring_merge(6, values, lse, s4, r4, y_peer)
    values, lse = ring_merge(7, values, lse, s5, r5, z_peer)

    wait(4, lambda d: wt.at[d], RING_ORDER[::-1])
    columns = wt[...].reshape(1024, 128)
    s6[...] = dot(values.astype(BF16), columns, ((1,), (1,))).astype(BF16)
    for slot in TP_ORDER:
        one = copy(8, s6, r6.at[me], slot, mirrored(slot), tp_peer(slot))
        one.start()
        sent.append(one)
    r6[me] = s6[...]
    for slot in TP_ORDER[::-1]:
        copy(8, s6, r6.at[0], slot, slot, tp_peer(1)).wait_recv()
    full = r6[0].astype(F32)
    for h in range(1, 8):
        full = full + r6[h].astype(F32)
    rms = lax.rsqrt(jnp.sum(full * full, axis=1, keepdims=True) / D + EPSILON)
    out[...] = (full[:, 0:16] * rms * ogain[...]).astype(BF16)
    for one in sent:
        one.wait_send()


def body(
    hidden_in, input_gain, down_query, down_latent, down_rope, query_gain, latent_gain, up_query, up_rope,
    key_up, value_up, out_proj, output_gain, latent_cache, rope_cache, lengths,
):
    operands = (
        hidden_in,
        input_gain.reshape(1, 128),
        down_query,
        down_latent,
        down_rope.T,
        query_gain.reshape(1, 256),
        latent_gain.reshape(1, 256),
        up_query.transpose(1, 0, 2).reshape(256, 128),
        up_rope.transpose(1, 2, 0).reshape(64, 256),
        key_up.transpose(1, 0, 2).reshape(256, 128),
        value_up.transpose(1, 0, 2).reshape(256, 128),
        out_proj.T,
        output_gain.reshape(1, 16),
        latent_cache,
        rope_cache.transpose(0, 2, 1),
    )
    loaded = [pltpu.VMEM(a.shape, a.dtype) for i, a in enumerate(operands) if i != 11]
    message = lambda *shape: pltpu.VMEM(shape, BF16)
    return pl.pallas_call(
        kernel,
        out_shape=jax.ShapeDtypeStruct((8, 16), BF16),
        in_specs=[pl.BlockSpec(memory_space=pltpu.SMEM)] + [pl.BlockSpec(memory_space=pl.ANY)] * len(operands),
        out_specs=pl.BlockSpec(memory_space=pltpu.VMEM),
        scratch_shapes=[
            *loaded,
            message(8, 384), message(8, 8, 384),
            message(8, 384), message(8, 8, 384),
            message(8, 384), message(8, 8, 384),
            message(8, 8, 384), message(8, 8, 384),
            message(8, 256), message(8, 8, 256),
            message(8, 256), message(8, 8, 256),
            message(8, 1024), message(8, 8, 1024),
            message(8, 8, 16, 128),
            pltpu.SemaphoreType.DMA((15,)),
            pltpu.SemaphoreType.DMA((9, 8)),
            pltpu.SemaphoreType.DMA((9, 8)),
        ],
        compiler_params=pltpu.CompilerParams(collective_id=0, has_side_effects=True),
    )(lengths, *operands)


def solution(mesh):
    split = Mesh(mesh.devices.reshape(8, 8, 4, 2), KV_TP)
    in_specs = (
        P(None, TP),
        P(TP),
        P(TP, None),
        P(TP, None),
        P(TP, None),
        P(),
        P(),
        P(None, TP, None),
        P(None, TP, None),
        P(None, TP, None),
        P(None, TP, None),
        P(TP, KV),
        P(KV),
        P(None, KV_TP, None),
        P(None, KV_TP, None),
        P(),
    )
    return jax.shard_map(body, mesh=split, in_specs=in_specs, out_specs=P(None, KV), check_vma=False)
```

time: 292 us -> 44.3 us (0.15); the launches traced: 286 us -> 44.2 us
  blocking collectives: 275 us -> 0 us
  Pallas kernels: 0 us -> 42.9 us
  other arithmetic: 4.91 us -> 0 us
    all_gather x13 -> x0, blocking collectives: 211 us -> none  [the longest x12 195 us: combined_by_axis(): pieces = jax.tree.map(lambda part: lax.all_gather(part, axis), x)]
    psum x4 -> x0, blocking collectives: 64.1 us -> none  [the longest x1 26.9 us: body(): lax.psum((local_sq, part_query, part_latent, part_rope), TP)]
    pallas_call x0 -> x1, Pallas kernels: none -> 42.9 us  [body(): pl.pallas_call(kernel, out_shape=jax.ShapeDtypeStruct((8, 16), BF16), in_...]
where the time goes in v1:
time: 44.3 us; the launch traced here: 44.2 us
  Pallas kernels  42.9 us (97%)
  local copies, waits for them, and re-layouts  1.26 us (3%)
    pallas_call x1, Pallas kernels, body(): pl.pallas_call(kernel, out_shape=jax.ShapeDtypeStruct((8, 16), BF16), in_...  42.9 us
    unnamed x1, local copies, waits for them, and re-layouts  1.26 us

profile of v1, /device:TPU:1, one launch (start us, length us, event | category | flops | bytes accessed | tf_op | source)
XLA Modules:
  0.0 44.2 jit_solution(6772889006806375323)
XLA Ops:
  0.0 42.9 %shard_map.154 = bf16[8,16]{1,0:T(8,128)(2,1)} custom-call(s32[8]{0:T(128)} %lengths.1, bf16[8,128]{1,0:T(8,128)(2,1)} %hidden_h.1, f32[1,128]{1,0:T(1,128)} %bitcast.22, bf16[128,256]{1,0:T(8,128)(2,1)} %dq_h.1, bf16[128,256]{1,0:T(8,128)(2,1)} %dl_h.1, bf16[64,128]{1,0:T(8,128)(2,1)} %bitcast.18, f32[1,256]{1,0:T(1,128)} %bitcast.20, f32[1,256]{1,0:T(1,128)} %bitcast.21, ...), custom_call_target="tpu_custom_call" | custom-call | tf_op jit(solution)/shard_map/pallas_call | solution.py:322
  42.9 1.3 %copy.18 = bf16[8,16]{1,0:T(8,128)(2,1)} copy(bf16[8,16]{1,0:T(8,128)(2,1)} %shard_map.154) | data formatting | bytes 512
